TPU v7x, 32 devices: a whole 2x2x4 slice. The times are simulated.
32 devices in a mesh: rep: 2 (over y), fs: 4 (over z), tp: 4 (over x, core).
Axes of the slice: x: 2, y: 2, z: 4, core: 2. Of those that a mesh axis runs over, the one named last changes fastest.
Arguments:
- tokens: bfloat16 [4096, 2048], P(('rep', 'fs'), 'tp'), may hold values from -6 to 6
- outer_gate: float32 [2048, 512], P('fs', 'tp'), may hold values from -0.125 to 0.125
- inner_gate: float32 [2048, 512], P('fs', 'tp'), may hold values from -0.125 to 0.125
- mixer_value: float32 [2048, 512], P('fs', 'tp'), may hold values from -0.125 to 0.125
- mixer_scales: float32 [3, 512], P(None, 'tp'), may hold values from 0.5 to 2
- mixer_taps: float32 [3, 512], P(None, 'tp'), may hold values from -3.5 to 3.5
- mixer_out: float32 [512, 2048], P('fs', 'tp'), may hold values from -0.25 to 0.25
- out_scale: float32 [2048], P('tp'), may hold values from 0.3 to 3
- first_gain: float32 [2048], replicated, may hold values from 0.1 to 1.9
- first_shift: float32 [2048], replicated, may hold values from -2 to 2
- up_proj: float32 [2048, 3072], P('fs', 'tp'), may hold values from -0.125 to 0.125
- gate_proj: float32 [2048, 3072], P('fs', 'tp'), may hold values from -0.125 to 0.125
- up_scales: float32 [2, 3072], P(None, 'tp'), may hold values from 0.5 to 2
- ffn_taps: float32 [3, 2, 3072], P(None, None, 'tp'), may hold values from -3.5 to 3.5
- ffn_shift: float32 [2, 3072], P(None, 'tp'), may hold values from -3 to 3
- down_proj: float32 [3072, 2048], P('fs', 'tp'), may hold values from -0.109375 to 0.109375
- down_scale: float32 [2048], P('tp'), may hold values from 0.3 to 3
- second_gain: float32 [2048], replicated, may hold values from 0.1 to 1.9
- second_shift: float32 [2048], replicated, may hold values from -2 to 2
Outputs:
- layer_out: bfloat16 [4096, 2048], P(('rep', 'fs'), 'tp')
All inputs are finite; a program needn't handle non-finite values.
Results may differ from a plain program's by a relative error of at most 0.017.
Values may be sent and summed in bfloat16 or wider, within the bound.
A program may use at most 64 MiB of HBM per device.

v0:
```python
import jax
import jax.numpy as jnp
from jax import lax
from jax.sharding import PartitionSpec as P

LEN = 128
norm_eps = 1e-05
residual_weight = 8.0**0.25


def causal_mix(signal, kernel_taps):
    sequences = signal.reshape(-1, LEN, signal.shape[-1])
    padded = jnp.pad(sequences, ((0, 0), (2, 0), (0, 0)))
    mixed = (
        kernel_taps[0] * padded[:, :-2]
        + kernel_taps[1] * padded[:, 1:-1]
        + kernel_taps[2] * padded[:, 2:]
    )
    return mixed.reshape(signal.shape)


def lowered(matrix):
    return matrix.astype(jnp.bfloat16)


def single_fold(operand, portion):
    return jnp.dot(operand, portion, preferred_element_type=jnp.float32)


def fold_step(operand, pieces):
    result = []
    for number in range(len(pieces)):
        result.append(jnp.dot(operand, pieces[number], preferred_element_type=jnp.float32))
    return tuple(result)


def own_columns(vector, own_width):
    return lax.dynamic_slice_in_dim(vector, lax.axis_index("tp") * own_width, own_width, 0)


def scaled_norm(summed, average, spread, gain_vector, shift_vector):
    return (summed - average) * lax.rsqrt(spread + norm_eps) * gain_vector + shift_vector


def local(
    tokens,
    outer_gate,
    inner_gate,
    mixer_value,
    mixer_scales,
    mixer_taps,
    mixer_out,
    out_scale,
    first_gain,
    first_shift,
    up_proj,
    gate_proj,
    up_scales,
    ffn_taps,
    ffn_shift,
    down_proj,
    down_scale,
    second_gain,
    second_shift,
):
    own_width = tokens.shape[1]
    full_width = own_width * lax.axis_size("tp")
    token_whole = lax.all_gather(tokens, "tp", axis=1, tiled=True)
    outer_part, inner_part, value_part = fold_step(
        token_whole,
        (
            lax.all_gather(lowered(outer_gate), "fs", axis=0, tiled=True),
            lax.all_gather(lowered(inner_gate), "fs", axis=0, tiled=True),
            lax.all_gather(lowered(mixer_value), "fs", axis=0, tiled=True),
        ),
    )
    outer_part = (outer_part * mixer_scales[0]).astype(jnp.bfloat16)
    inner_part = (inner_part * mixer_scales[1]).astype(jnp.bfloat16)
    value_part = (value_part * mixer_scales[2]).astype(jnp.bfloat16)
    product = inner_part.astype(jnp.float32) * value_part.astype(jnp.float32)
    mixed_conv = (outer_part.astype(jnp.float32) * causal_mix(product, mixer_taps)).astype(
        jnp.bfloat16
    )
    conv_whole = lax.all_gather(mixed_conv, "tp", axis=1, tiled=True)
    mixer_sum = (
        single_fold(conv_whole, lax.all_gather(lowered(mixer_out), "fs", axis=0, tiled=True))
        * out_scale
    )
    first_sum = residual_weight * tokens.astype(jnp.float32) + mixer_sum
    row_total, row_square = lax.psum(
        (jnp.sum(first_sum, 1, keepdims=True), jnp.sum(first_sum * first_sum, 1, keepdims=True)),
        "tp",
    )
    average = row_total / full_width
    spread = row_square / full_width - average * average
    normed = scaled_norm(
        first_sum,
        average,
        spread,
        own_columns(first_gain, own_width),
        own_columns(first_shift, own_width),
    ).astype(jnp.bfloat16)
    normed_whole = lax.all_gather(normed, "tp", axis=1, tiled=True)
    up_matrix, gate_matrix = (
        lax.all_gather(lowered(up_proj), "fs", axis=0, tiled=True),
        lax.all_gather(lowered(gate_proj), "fs", axis=0, tiled=True),
    )
    up_linear = jnp.dot(normed_whole, up_matrix, preferred_element_type=jnp.float32)
    gate_linear = jnp.dot(normed_whole, gate_matrix, preferred_element_type=jnp.float32)
    up_linear = up_linear * up_scales[0]
    gate_linear = gate_linear * up_scales[1]
    up_mixed = causal_mix(up_linear, ffn_taps[:, 0]) + ffn_shift[0]
    gate_mixed = causal_mix(gate_linear, ffn_taps[:, 1]) + ffn_shift[1]
    hidden = (up_mixed * jax.nn.silu(gate_mixed)).astype(jnp.bfloat16)
    hidden_whole = lax.all_gather(hidden, "tp", axis=1, tiled=True)
    ffn_sum = (
        single_fold(hidden_whole, lax.all_gather(lowered(down_proj), "fs", axis=0, tiled=True))
        * down_scale
    )
    second_sum = residual_weight * normed.astype(jnp.float32) + ffn_sum
    second_total, second_square = lax.psum(
        (jnp.sum(second_sum, 1, keepdims=True), jnp.sum(second_sum * second_sum, 1, keepdims=True)),
        "tp",
    )
    second_average = second_total / full_width
    second_spread = second_square / full_width - second_average * second_average
    return scaled_norm(
        second_sum,
        second_average,
        second_spread,
        own_columns(second_gain, own_width),
        own_columns(second_shift, own_width),
    ).astype(jnp.bfloat16)


def solution(mesh):
    return jax.shard_map(
        local,
        mesh=mesh,
        in_specs=(
            P(("rep", "fs"), "tp"),
            P("fs", "tp"),
            P("fs", "tp"),
            P("fs", "tp"),
            P(None, "tp"),
            P(None, "tp"),
            P("fs", "tp"),
            P("tp"),
            P(),
            P(),
            P("fs", "tp"),
            P("fs", "tp"),
            P(None, "tp"),
            P(None, None, "tp"),
            P(None, "tp"),
            P("fs", "tp"),
            P("tp"),
            P(),
            P(),
        ),
        out_specs=P(("rep", "fs"), "tp"),
        check_vma=False,
    )
```

profile of v0, /device:TPU:0, one launch (start us, length us, event | category | flops | bytes accessed | tf_op | source)
XLA Modules:
  0.0 314.0 jit_solution(7180715300881190758)
XLA Ops:
  6.5 0.7 all-gather.7.cloned.1.call-update
  7.3 0.0 all-gather.11.cloned.1.call-start
  7.3 2.4 convert_element_type.76
  9.8 0.0 all-gather.11.cloned.1.call-update
  9.8 0.0 all-gather.9.cloned.1.call-start
  9.9 1.0 copy.22
  11.0 0.0 copy-start.13
  11.0 0.8 dynamic_slice.12
  11.8 0.8 dynamic_slice.13
  12.5 17.4 %all_gather.36 = bf16[2048,128]{1,0:T(8,128)(2,1)S(1)} all-gather(bf16[512,128]{1,0:T(8,128)(2,1)S(1)} %convert_element_type.69), channel_id=1, replica_groups=mesh['rep'=2,'fs'=4,'tp'=4] {'fs'}, dimensions={0}, use_global_device_ids=true | all-gather | bytes 655360 | tf_op jit(solution)/shard_map/all_gather | solution.py:74
  29.9 16.9 %all_gather.35 = bf16[2048,128]{1,0:T(8,128)(2,1)S(1)} all-gather(bf16[512,128]{1,0:T(8,128)(2,1)S(1)} %convert_element_type.66), channel_id=1, replica_groups=mesh['rep'=2,'fs'=4,'tp'=4] {'fs'}, dimensions={0}, use_global_device_ids=true | all-gather | bytes 655360 | tf_op jit(solution)/shard_map/all_gather | solution.py:73
  46.8 22.6 %all_gather.34 = bf16[2048,128]{1,0:T(8,128)(2,1)S(1)} all-gather(bf16[512,128]{1,0:T(8,128)(2,1)S(1)} %convert_element_type.63), channel_id=1, replica_groups=mesh['rep'=2,'fs'=4,'tp'=4] {'fs'}, dimensions={0}, use_global_device_ids=true | all-gather | bytes 655360 | tf_op jit(solution)/shard_map/all_gather | solution.py:72
  69.4 20.2 %all_gather.38 = bf16[512,512]{1,0:T(8,128)(2,1)S(1)} all-gather(bf16[128,512]{1,0:T(8,128)(2,1)S(1)} %convert_element_type.73), channel_id=1, replica_groups=mesh['rep'=2,'fs'=4,'tp'=4] {'fs'}, dimensions={0}, use_global_device_ids=true | all-gather | bytes 655360 | tf_op jit(solution)/shard_map/all_gather | solution.py:86
  89.6 0.0 all-gather.7.cloned.1.call-done
  89.6 2.5 fusion.20
  92.1 0.7 fusion.18
  92.8 0.1 fusion.23
  92.9 0.7 fusion.15
  93.7 7.0 %all_gather.37 = bf16[512,512]{1,0:T(8,128)(2,1)S(1)} all-gather(bf16[512,128]{1,0:T(8,128)(2,1)S(1)} %fusion.15), channel_id=1, replica_groups=mesh['rep'=2,'fs'=4,'tp'=4] {'tp'}, dimensions={1}, use_global_device_ids=true | all-gather | bytes 655360 | tf_op jit(solution)/shard_map/all_gather | solution.py:84
  100.7 0.6 fusion.26
  101.3 7.0 %all-reduce.4 = (f32[512,1]{0,1:T(1,128)S(1)}, f32[512,1]{0,1:T(1,128)S(1)}) all-reduce(f32[512,1]{0,1:T(1,128)S(1)} %bitcast.57, f32[512,1]{0,1:T(1,128)S(1)} %bitcast.56), channel_id=1, replica_groups=mesh['rep'=2,'fs'=4,'tp'=4] {'tp'}, use_global_device_ids=true, to_apply=%region_3.4 | all-reduce | flops 1024 | bytes 8192 | tf_op jit(solution)/shard_map/psum | solution.py:90
  108.3 1.0 add_convert_fusion.1
  109.3 0.0 all-gather.9.cloned.1.call-update
  109.3 0.0 all-gather.13.cloned.1.call-start
  109.4 1.0 convert_element_type.77
  110.4 0.0 all-gather.13.cloned.1.call-update
  110.5 0.0 all-gather.17.cloned.1.call-start
  110.5 0.5 copy-done.4
  111.0 1.0 convert_element_type.79
  112.0 0.0 all-gather.17.cloned.1.call-update
  112.0 0.0 all-gather.15.cloned.1.call-start
  112.1 0.1 slice_reduce_fusion.4
  112.2 2.2 all-gather.11.cloned.1.call-done
  114.4 23.7 %all-gather.9.cloned.1.call-done = bf16[512,2048]{0,1:T(8,128)(2,1)} async-done(((bf16[512,512]{0,1:T(8,128)(2,1)}), bf16[512,2048]{0,1:T(8,128)(2,1)}) %all-gather.9.cloned.1.call-update) | async-done | bytes 2097168 | tf_op jit(solution)/shard_map/all_gather | solution.py:103
  138.2 4.4 %convolution_multiply_fusion.1 = f32[512,768]{1,0:T(8,128)S(1)} fusion(bf16[512,2048]{0,1:T(8,128)(2,1)} %all-gather.9.cloned.1.call-done, bf16[2048,768]{1,0:T(8,128)(2,1)} %all-gather.11.cloned.1.call-done, f32[768]{0:T(1024)S(1)} %get-tuple-element.18), kind=kOutput, calls=%fused_computation.17 | convolution fusion | flops 1611005952 | bytes 6818816 | tf_op jit(solution)/shard_map/dot_general | solution.py:108
  142.5 60.5 %all-gather.13.cloned.1.call-done = bf16[2048,768]{1,0:T(8,128)(2,1)} async-done(((bf16[512,768]{1,0:T(8,128)(2,1)}), bf16[2048,768]{1,0:T(8,128)(2,1)}) %all-gather.13.cloned.1.call-update) | async-done | bytes 3145744 | tf_op jit(solution)/shard_map/all_gather | solution.py:106
  203.1 4.4 %convolution_multiply_fusion = f32[512,768]{1,0:T(8,128)S(1)} fusion(bf16[512,2048]{0,1:T(8,128)(2,1)} %all-gather.9.cloned.1.call-done, bf16[2048,768]{1,0:T(8,128)(2,1)} %all-gather.13.cloned.1.call-done, f32[768]{0:T(1024)S(1)} %get-tuple-element.17), kind=kOutput, calls=%fused_computation.16 | convolution fusion | flops 1611005952 | bytes 6818816 | tf_op jit(solution)/shard_map/dot_general | solution.py:109
  207.4 0.9 fusion.2
  208.4 1.4 fusion.9
  209.8 0.0 all-gather.15.cloned.1.call-update
  209.8 0.8 dynamic_slice.14
  210.5 0.8 dynamic_slice.15
  211.3 55.3 %all-gather.17.cloned.1.call-done = bf16[3072,512]{1,0:T(8,128)(2,1)} async-done(((bf16[768,512]{1,0:T(8,128)(2,1)}), bf16[3072,512]{1,0:T(8,128)(2,1)}) %all-gather.17.cloned.1.call-update) | async-done | bytes 3145744 | tf_op jit(solution)/shard_map/all_gather | solution.py:117
  266.6 28.6 %all-gather.15.cloned.1.call-done = bf16[512,3072]{1,0:T(8,128)(2,1)} async-done(((bf16[512,768]{1,0:T(8,128)(2,1)}), bf16[512,3072]{1,0:T(8,128)(2,1)}) %all-gather.15.cloned.1.call-update) | async-done | bytes 3145744 | tf_op jit(solution)/shard_map/all_gather | solution.py:115
  295.2 4.8 %fusion.25 = (f32[512]{0:T(512)S(1)}, f32[512]{0:T(512)S(1)}, f32[512,512]{0,1:T(8,128)S(1)}) fusion(f32[512]{0:T(512)S(1)} %copy-done.16, bf16[512,3072]{1,0:T(8,128)(2,1)} %all-gather.15.cloned.1.call-done, bf16[3072,512]{1,0:T(8,128)(2,1)} %all-gather.17.cloned.1.call-done, bf16[512,512]{0,1:T(8,128)(2,1)S(1)} %copy-done.1), kind=kOutput, calls=%fused_computation.64 | convolution fusion | flops 1612446720 | bytes 7870464 | tf_op jit(solution)/shard_map/dot_general | solution.py:27
  300.0 5.9 %all-reduce.3 = (f32[512,1]{0,1:T(1,128)S(1)}, f32[512,1]{0,1:T(1,128)S(1)}) all-reduce(f32[512,1]{0,1:T(1,128)S(1)} %bitcast.59, f32[512,1]{0,1:T(1,128)S(1)} %bitcast.58), channel_id=1, replica_groups=mesh['rep'=2,'fs'=4,'tp'=4] {'tp'}, use_global_device_ids=true, to_apply=%region_7.8 | all-reduce | flops 1024 | bytes 8192 | tf_op jit(solution)/shard_map/psum | solution.py:121
  305.9 0.2 add_convert_fusion
  306.1 1.0 copy.23
  (43 shorter events, 0.2 us)
Async XLA Ops:
  6.5 83.1 %all-gather.7.cloned.1.call-start = ((), (), s32[]{:S(2)}) async-start(), calls=%async_computation | async-start | bytes 2621440 | tf_op jit(solution)/shard_map/all_gather | solution.py:68
  7.3 2.6 copy-start.2
  7.3 3.6 %copy-start.6 = (f32[512,128]{1,0:T(8,128)S(1)}, f32[512,128]{1,0:T(8,128)}, u32[]{:S(2)}) copy-start(f32[512,128]{1,0:T(8,128)} %param.22) | copy-start | bytes 786436
  7.3 107.2 %all-gather.11.cloned.1.call-start = ((), (), s32[]{:S(2)}) async-start(), calls=%async_computation.2 | async-start | bytes 3932160 | tf_op jit(solution)/shard_map/all_gather | solution.py:105
  9.8 1.1 copy-start.7
  9.8 1.2 copy-start.8
  9.8 1.2 copy-start.9
  9.8 128.4 %all-gather.9.cloned.1.call-start = ((), (), s32[]{:S(2)}) async-start(), calls=%async_computation.1 | async-start | bytes 2621440 | tf_op jit(solution)/shard_map/all_gather | solution.py:103
  11.0 78.6 %copy-start.13 = (f32[3,128]{1,0:T(4,128)S(1)}, f32[3,128]{1,0:T(4,128)}, u32[]{:S(2)}) copy-start(f32[3,128]{1,0:T(4,128)} %param.23) | copy-start | bytes 4612
  11.0 78.6 %copy-start.14 = (f32[3,128]{1,0:T(4,128)S(1)}, f32[3,128]{1,0:T(4,128)}, u32[]{:S(2)}) copy-start(f32[3,128]{1,0:T(4,128)} %param.24) | copy-start | bytes 4612
  89.6 2.5 copy-start
  92.9 7.8 %copy-start.5 = (bf16[512,512]{0,1:T(8,128)(2,1)S(1)}, bf16[512,512]{0,1:T(8,128)(2,1)}, u32[]{:S(2)}) copy-start(bf16[512,512]{0,1:T(8,128)(2,1)} %copy.22) | copy-start | bytes 1572868
  92.9 7.8 %copy-start.15 = (f32[512]{0:T(512)S(1)}, f32[512]{0:T(512)}, u32[]{:S(2)}) copy-start(f32[512]{0:T(512)} %param.26) | copy-start | bytes 6148
  101.3 8.1 %copy-start.3 = (f32[512,768]{1,0:T(8,128)S(1)}, f32[512,768]{1,0:T(8,128)}, u32[]{:S(2)}) copy-start(f32[512,768]{1,0:T(8,128)} %param.30) | copy-start | bytes 4718596
  109.3 1.7 copy-start.4
  109.3 93.8 %all-gather.13.cloned.1.call-start = ((), (), s32[]{:S(2)}) async-start(), calls=%async_computation.3 | async-start | bytes 3932160 | tf_op jit(solution)/shard_map/all_gather | solution.py:106
  110.4 1.6 copy-start.11
  110.4 1.7 copy-start.12
  110.4 1.7 copy-start.10
  110.5 156.2 %all-gather.17.cloned.1.call-start = ((), (), s32[]{:S(2)}) async-start(), calls=%async_computation.5 | async-start | bytes 3932160 | tf_op jit(solution)/shard_map/all_gather | solution.py:117
  112.0 183.2 %all-gather.15.cloned.1.call-start = ((), (), s32[]{:S(2)}) async-start(), calls=%async_computation.4 | async-start | bytes 3932160 | tf_op jit(solution)/shard_map/all_gather | solution.py:115
  208.4 86.8 %copy-start.1 = (bf16[512,512]{0,1:T(8,128)(2,1)S(1)}, bf16[512,512]{0,1:T(8,128)(2,1)}, u32[]{:S(2)}) copy-start(bf16[512,512]{0,1:T(8,128)(2,1)} %add_convert_fusion.1) | copy-start | bytes 1572868
  208.4 86.8 %copy-start.16 = (f32[512]{0:T(512)S(1)}, f32[512]{0:T(512)}, u32[]{:S(2)}) copy-start(f32[512]{0:T(512)} %param.35) | copy-start | bytes 6148
Sparse Core Ops, SparseCore 0:
  8.9 25.2 all-gather.6
  35.8 78.6 all-gather.10
  116.0 22.1 all-gather.8
  139.6 63.4 all-gather.12
  204.5 62.0 all-gather.16
  268.0 27.1 all-gather.14
where the time goes:
time: 314 us
  waiting for transfers between devices  171 us (54%)
  blocking collectives  96.9 us (31%)
  matrix products  18 us (6%)
  between operations  13.8 us (4%)
  other arithmetic  8.13 us (3%)
  local copies, waits for them, and re-layouts  5.76 us (2%)
    all_gather x1, waiting for transfers between devices, local(): lax.all_gather(lowered(gate_proj), 'fs', axis=0, tiled=True)  60.5 us
    all_gather x1, waiting for transfers between devices, local(): lax.all_gather(lowered(down_proj), 'fs', axis=0, tiled=True)  55.3 us
    all_gather x1, waiting for transfers between devices, local(): hidden_whole = lax.all_gather(hidden, 'tp', axis=1, tiled=True)  28.6 us
    all_gather x1, waiting for transfers between devices, local(): normed_whole = lax.all_gather(normed, 'tp', axis=1, tiled=True)  23.7 us
    all_gather x1, blocking collectives, local(): lax.all_gather(lowered(outer_gate), 'fs', axis=0, tiled=True)  22.6 us
    all_gather x1, blocking collectives, local(): lax.all_gather(lowered(mixer_out), 'fs', axis=0, tiled=True)  20.2 us
    all_gather x1, blocking collectives, local(): lax.all_gather(lowered(mixer_value), 'fs', axis=0, tiled=True)  17.4 us
    all_gather x1, blocking collectives, local(): lax.all_gather(lowered(inner_gate), 'fs', axis=0, tiled=True)  16.9 us
  transfers between devices with their start and end apart: 6, of which 5 were waited for; matrix products, arithmetic and copies ran while one was open for 8% of the time, Pallas kernels for 0%

commit v1 on v0

--- a/solution.py
+++ b/solution.py
@@ -112,7 +112,12 @@
     up_mixed = causal_mix(up_linear, ffn_taps[:, 0]) + ffn_shift[0]
     gate_mixed = causal_mix(gate_linear, ffn_taps[:, 1]) + ffn_shift[1]
     hidden = (up_mixed * jax.nn.silu(gate_mixed)).astype(jnp.bfloat16)
-    hidden_whole = lax.all_gather(hidden, "tp", axis=1, tiled=True)
+    ring = [hidden]
+    for hop in range(3):
+        ring.append(lax.ppermute(ring[-1], "tp", [(dev, (dev + 1) % 4) for dev in range(4)]))
+    hidden_whole = jnp.roll(
+        jnp.concatenate(ring[::-1], axis=1), (lax.axis_index("tp") + 1) * ring[0].shape[1], axis=1
+    )
     ffn_sum = (
         single_fold(hidden_whole, lax.all_gather(lowered(down_proj), "fs", axis=0, tiled=True))
         * down_scale

time: 314 us -> 286 us (0.911)
  waiting for transfers between devices: 171 us -> 136 us
  local copies, waits for them, and re-layouts: 5.76 us -> 13.7 us
    all_gather x1, waiting for transfers between devices: 55.3 us -> 15.5 us  [local(): lax.all_gather(lowered(down_proj), 'fs', axis=0, tiled=True)]
    ppermute x0 -> x3, waiting for transfers between devices: none -> 32.7 us  [local(): lax.ppermute(ring[-1], 'tp', [(dev, (dev + 1) % 4) for dev in range(4)])]
    all_gather x1 -> x0, waiting for transfers between devices: 28.6 us -> none  [local(): hidden_whole = lax.all_gather(hidden, 'tp', axis=1, tiled=True)]
    unnamed x35 -> x42, local copies, waits for them, and re-layouts: 1.59 us -> 8.51 us
  transfers between devices with their start and end apart: 6 -> 8, of which waited for: 5 -> 7; matrix products, arithmetic and copies ran while one was open for 8% -> 11% of each run, Pallas kernels for 0% -> 0%
where the time goes in v1:
time: 286 us
  waiting for transfers between devices  136 us (48%)
  blocking collectives  97.3 us (34%)
  matrix products  18.4 us (6%)
  local copies, waits for them, and re-layouts  13.7 us (5%)
  between operations  13.4 us (5%)
  other arithmetic  7.24 us (3%)
    all_gather x1, waiting for transfers between devices, local(): lax.all_gather(lowered(gate_proj), 'fs', axis=0, tiled=True)  60.5 us
    ppermute x3, waiting for transfers between devices, local(): lax.ppermute(ring[-1], 'tp', [(dev, (dev + 1) % 4) for dev in range(4)])  32.7 us
    all_gather x1, waiting for transfers between devices, local(): normed_whole = lax.all_gather(normed, 'tp', axis=1, tiled=True)  23.7 us
    all_gather x1, blocking collectives, local(): lax.all_gather(lowered(outer_gate), 'fs', axis=0, tiled=True)  22.5 us
    all_gather x1, blocking collectives, local(): lax.all_gather(lowered(mixer_out), 'fs', axis=0, tiled=True)  20.2 us
    all_gather x1, blocking collectives, local(): lax.all_gather(lowered(mixer_value), 'fs', axis=0, tiled=True)  17.4 us
    all_gather x1, blocking collectives, local(): lax.all_gather(lowered(inner_gate), 'fs', axis=0, tiled=True)  16.9 us
    all_gather x1, waiting for transfers between devices, local(): lax.all_gather(lowered(down_proj), 'fs', axis=0, tiled=True)  15.5 us
  transfers between devices with their start and end apart: 8, of which 7 were waited for; matrix products, arithmetic and copies ran while one was open for 11% of the time, Pallas kernels for 0%

profile of v1, /device:TPU:0, one launch (start us, length us, event | category | flops | bytes accessed | tf_op | source)
XLA Modules:
  0.0 285.9 jit_solution(7963090939256901115)
XLA Ops:
  6.5 0.7 all-gather.6.cloned.1.call-update
  7.3 2.4 convert_element_type.76
  9.8 0.0 all-gather.8.cloned.1.call-start
  9.9 1.0 copy.22
  11.0 0.8 dynamic_slice.16
  11.8 0.8 dynamic_slice.17
  12.5 17.4 %all_gather.33 = bf16[2048,128]{1,0:T(8,128)(2,1)S(1)} all-gather(bf16[512,128]{1,0:T(8,128)(2,1)S(1)} %convert_element_type.69), channel_id=1, replica_groups=mesh['rep'=2,'fs'=4,'tp'=4] {'fs'}, dimensions={0}, use_global_device_ids=true | all-gather | bytes 655360 | tf_op jit(solution)/shard_map/all_gather | solution.py:74
  29.9 16.9 %all_gather.32 = bf16[2048,128]{1,0:T(8,128)(2,1)S(1)} all-gather(bf16[512,128]{1,0:T(8,128)(2,1)S(1)} %convert_element_type.66), channel_id=1, replica_groups=mesh['rep'=2,'fs'=4,'tp'=4] {'fs'}, dimensions={0}, use_global_device_ids=true | all-gather | bytes 655360 | tf_op jit(solution)/shard_map/all_gather | solution.py:73
  46.8 22.5 %all_gather.31 = bf16[2048,128]{1,0:T(8,128)(2,1)S(1)} all-gather(bf16[512,128]{1,0:T(8,128)(2,1)S(1)} %convert_element_type.63), channel_id=1, replica_groups=mesh['rep'=2,'fs'=4,'tp'=4] {'fs'}, dimensions={0}, use_global_device_ids=true | all-gather | bytes 655360 | tf_op jit(solution)/shard_map/all_gather | solution.py:72
  69.3 20.2 %all_gather.35 = bf16[512,512]{1,0:T(8,128)(2,1)S(1)} all-gather(bf16[128,512]{1,0:T(8,128)(2,1)S(1)} %convert_element_type.73), channel_id=1, replica_groups=mesh['rep'=2,'fs'=4,'tp'=4] {'fs'}, dimensions={0}, use_global_device_ids=true | all-gather | bytes 655360 | tf_op jit(solution)/shard_map/all_gather | solution.py:86
  89.6 2.5 fusion.27
  92.1 0.7 fusion.25
  92.8 0.1 fusion.30
  92.9 0.7 fusion.22
  93.6 7.1 %all_gather.34 = bf16[512,512]{1,0:T(8,128)(2,1)S(1)} all-gather(bf16[512,128]{1,0:T(8,128)(2,1)S(1)} %fusion.22), channel_id=1, replica_groups=mesh['rep'=2,'fs'=4,'tp'=4] {'tp'}, dimensions={1}, use_global_device_ids=true | all-gather | bytes 655360 | tf_op jit(solution)/shard_map/all_gather | solution.py:84
  100.7 0.6 fusion.34
  101.3 6.8 %all-reduce.4 = (f32[512,1]{0,1:T(1,128)S(1)}, f32[512,1]{0,1:T(1,128)S(1)}) all-reduce(f32[512,1]{0,1:T(1,128)S(1)} %bitcast.58, f32[512,1]{0,1:T(1,128)S(1)} %bitcast.57), channel_id=1, replica_groups=mesh['rep'=2,'fs'=4,'tp'=4] {'tp'}, use_global_device_ids=true, to_apply=%region_3.4 | all-reduce | flops 1024 | bytes 8192 | tf_op jit(solution)/shard_map/psum | solution.py:90
  108.2 1.0 add_convert_fusion.1
  109.2 1.0 convert_element_type.77
  110.3 0.5 copy-done.4
  110.9 1.0 convert_element_type.79
  111.9 0.1 slice_reduce_fusion.4
  112.0 2.4 all-gather.10.cloned.1.call-done
  114.4 23.7 %all-gather.8.cloned.1.call-done = bf16[512,2048]{0,1:T(8,128)(2,1)} async-done(((bf16[512,512]{0,1:T(8,128)(2,1)}), bf16[512,2048]{0,1:T(8,128)(2,1)}) %all-gather.8.cloned.1.call-update) | async-done | bytes 2097168 | tf_op jit(solution)/shard_map/all_gather | solution.py:103
  138.2 4.4 %convolution_multiply_fusion.1 = f32[512,768]{1,0:T(8,128)S(1)} fusion(bf16[512,2048]{0,1:T(8,128)(2,1)} %all-gather.8.cloned.1.call-done, bf16[2048,768]{1,0:T(8,128)(2,1)} %all-gather.10.cloned.1.call-done, f32[768]{0:T(1024)S(1)} %get-tuple-element.18), kind=kOutput, calls=%fused_computation.19 | convolution fusion | flops 1611005952 | bytes 6818816 | tf_op jit(solution)/shard_map/dot_general | solution.py:108
  142.5 60.5 %all-gather.12.cloned.1.call-done = bf16[2048,768]{1,0:T(8,128)(2,1)} async-done(((bf16[512,768]{1,0:T(8,128)(2,1)}), bf16[2048,768]{1,0:T(8,128)(2,1)}) %all-gather.12.cloned.1.call-update) | async-done | bytes 3145744 | tf_op jit(solution)/shard_map/all_gather | solution.py:106
  203.1 4.4 %convolution_multiply_fusion = f32[512,768]{1,0:T(8,128)S(1)} fusion(bf16[512,2048]{0,1:T(8,128)(2,1)} %all-gather.8.cloned.1.call-done, bf16[2048,768]{1,0:T(8,128)(2,1)} %all-gather.12.cloned.1.call-done, f32[768]{0:T(1024)S(1)} %get-tuple-element.17), kind=kOutput, calls=%fused_computation.18 | convolution fusion | flops 1611005952 | bytes 6818816 | tf_op jit(solution)/shard_map/dot_general | solution.py:109
  207.4 0.9 fusion.4
  208.4 0.5 fusion.11
  208.8 0.1 collective-permute-start
  208.9 11.4 %collective-permute-done = bf16[512,768]{1,0:T(8,128)(2,1)S(1)} collective-permute-done((bf16[512,768]{1,0:T(8,128)(2,1)S(1)}, bf16[512,768]{1,0:T(8,128)(2,1)S(1)}, u32[]{:S(2)}, u32[]{:S(2)}) %collective-permute-start) | collective-permute-done | bytes 786464 | tf_op jit(solution)/shard_map/ppermute | solution.py:117
  220.3 11.4 %collective-permute-done.1 = bf16[512,768]{1,0:T(8,128)(2,1)S(1)} collective-permute-done((bf16[512,768]{1,0:T(8,128)(2,1)S(1)}, bf16[512,768]{1,0:T(8,128)(2,1)S(1)}, u32[]{:S(2)}, u32[]{:S(2)}) %collective-permute-start.1) | collective-permute-done | bytes 786464 | tf_op jit(solution)/shard_map/ppermute | solution.py:117
  231.7 0.8 dynamic_slice.19
  232.5 0.8 dynamic_slice.20
  233.2 9.9 %collective-permute-done.2 = bf16[512,768]{1,0:T(8,128)(2,1)S(1)} collective-permute-done((bf16[512,768]{1,0:T(8,128)(2,1)S(1)}, bf16[512,768]{1,0:T(8,128)(2,1)S(1)}, u32[]{:S(2)}, u32[]{:S(2)}) %collective-permute-start.2) | collective-permute-done | bytes 786464 | tf_op jit(solution)/shard_map/ppermute | solution.py:117
  243.1 1.0 constant_dynamic-update-slice_fusion.7
  244.1 1.0 constant_dynamic-update-slice_fusion.6
  245.1 1.0 constant_dynamic-update-slice_fusion.5
  246.1 1.0 constant_dynamic-update-slice_fusion.4
  247.0 1.0 constant_dynamic-update-slice_fusion.3
  248.1 1.0 constant_dynamic-update-slice_fusion.2
  249.1 1.0 constant_dynamic-update-slice_fusion.1
  250.1 1.0 constant_dynamic-update-slice_fusion
  251.1 15.5 %all-gather.14.cloned.1.call-done = bf16[3072,512]{1,0:T(8,128)(2,1)} async-done(((bf16[768,512]{1,0:T(8,128)(2,1)}), bf16[3072,512]{1,0:T(8,128)(2,1)}) %all-gather.14.cloned.1.call-update) | async-done | bytes 3145744 | tf_op jit(solution)/shard_map/all_gather | solution.py:122
  266.6 5.2 %fusion.33 = (f32[512]{0:T(512)S(1)}, f32[512]{0:T(512)S(1)}, f32[512,512]{0,1:T(8,128)S(1)}) fusion(f32[512]{0:T(512)S(1)} %copy-done.16, bf16[3072,512]{1,0:T(8,128)(2,1)} %all-gather.14.cloned.1.call-done, bf16[512,6144]{1,0:T(8,128)(2,1)} %constant_dynamic-update-slice_fusion, s32[]{:T(128)S(6)} %select_n.21, bf16[512,512]{0,1:T(8,128)(2,1)S(1)} %copy-done.1), kind=kOutput, calls=%fused_computation.75 | convolution fusion | flops 1612446720 | bytes 7870468 | tf_op jit(solution)/shard_map/dot_general | solution.py:27
  271.8 6.4 %all-reduce.3 = (f32[512,1]{0,1:T(1,128)S(1)}, f32[512,1]{0,1:T(1,128)S(1)}) all-reduce(f32[512,1]{0,1:T(1,128)S(1)} %bitcast.56, f32[512,1]{0,1:T(1,128)S(1)} %bitcast.55), channel_id=1, replica_groups=mesh['rep'=2,'fs'=4,'tp'=4] {'tp'}, use_global_device_ids=true, to_apply=%region_7.8 | all-reduce | flops 1024 | bytes 8192 | tf_op jit(solution)/shard_map/psum | solution.py:126
  278.2 0.2 add_convert_fusion
  278.4 1.0 copy.23
  (54 shorter events, 0.4 us)
Async XLA Ops:
  6.5 3.3 %copy-start.2 = (bf16[512,512]{1,0:T(8,128)(2,1)S(1)}, bf16[512,512]{1,0:T(8,128)(2,1)}, u32[]{:S(2)}) copy-start(bf16[512,512]{1,0:T(8,128)(2,1)} %param.19) | copy-start | bytes 1572868
  6.5 83.1 %all-gather.6.cloned.1.call-start = ((), (), s32[]{:S(2)}) async-start(), calls=%async_computation | async-start | bytes 2621440 | tf_op jit(solution)/shard_map/all_gather | solution.py:68
  7.3 3.6 %copy-start.6 = (f32[512,128]{1,0:T(8,128)S(1)}, f32[512,128]{1,0:T(8,128)}, u32[]{:S(2)}) copy-start(f32[512,128]{1,0:T(8,128)} %param.22) | copy-start | bytes 786436
  7.3 3.6 %copy-start.7 = (f32[512,128]{1,0:T(8,128)S(1)}, f32[512,128]{1,0:T(8,128)}, u32[]{:S(2)}) copy-start(f32[512,128]{1,0:T(8,128)} %param.21) | copy-start | bytes 786436
  7.3 3.7 %copy-start.8 = (f32[512,128]{1,0:T(8,128)S(1)}, f32[512,128]{1,0:T(8,128)}, u32[]{:S(2)}) copy-start(f32[512,128]{1,0:T(8,128)} %param.20) | copy-start | bytes 786436
  7.3 107.2 %all-gather.10.cloned.1.call-start = ((), (), s32[]{:S(2)}) async-start(), calls=%async_computation.2 | async-start | bytes 3932160 | tf_op jit(solution)/shard_map/all_gather | solution.py:105
  9.8 1.2 copy-start.9
  9.8 128.3 %all-gather.8.cloned.1.call-start = ((), (), s32[]{:S(2)}) async-start(), calls=%async_computation.1 | async-start | bytes 2621440 | tf_op jit(solution)/shard_map/all_gather | solution.py:103
  10.9 78.7 %copy-start.13 = (f32[3,128]{1,0:T(4,128)S(1)}, f32[3,128]{1,0:T(4,128)}, u32[]{:S(2)}) copy-start(f32[3,128]{1,0:T(4,128)} %param.23) | copy-start | bytes 4612
  10.9 78.7 %copy-start.14 = (f32[3,128]{1,0:T(4,128)S(1)}, f32[3,128]{1,0:T(4,128)}, u32[]{:S(2)}) copy-start(f32[3,128]{1,0:T(4,128)} %param.24) | copy-start | bytes 4612
  89.6 2.5 copy-start
  92.8 7.9 %copy-start.5 = (bf16[512,512]{0,1:T(8,128)(2,1)S(1)}, bf16[512,512]{0,1:T(8,128)(2,1)}, u32[]{:S(2)}) copy-start(bf16[512,512]{0,1:T(8,128)(2,1)} %copy.22) | copy-start | bytes 1572868
  92.8 7.9 %copy-start.15 = (f32[512]{0:T(512)S(1)}, f32[512]{0:T(512)}, u32[]{:S(2)}) copy-start(f32[512]{0:T(512)} %param.26) | copy-start | bytes 6148
  100.7 8.5 %copy-start.3 = (f32[512,768]{1,0:T(8,128)S(1)}, f32[512,768]{1,0:T(8,128)}, u32[]{:S(2)}) copy-start(f32[512,768]{1,0:T(8,128)} %param.30) | copy-start | bytes 4718596
  109.2 1.7 copy-start.4
  109.2 93.9 %all-gather.12.cloned.1.call-start = ((), (), s32[]{:S(2)}) async-start(), calls=%async_computation.3 | async-start | bytes 3932160 | tf_op jit(solution)/shard_map/all_gather | solution.py:106
  110.3 1.6 copy-start.11
  110.3 1.6 copy-start.10
  110.3 1.7 copy-start.12
  110.3 156.3 %all-gather.14.cloned.1.call-start = ((), (), s32[]{:S(2)}) async-start(), calls=%async_computation.4 | async-start | bytes 3932160 | tf_op jit(solution)/shard_map/all_gather | solution.py:122
  208.8 11.5 %collective-permute-start = (bf16[512,768]{1,0:T(8,128)(2,1)S(1)}, bf16[512,768]{1,0:T(8,128)(2,1)S(1)}, u32[]{:S(2)}, u32[]{:S(2)}) collective-permute-start(bf16[512,768]{1,0:T(8,128)(2,1)S(1)} %fusion.11), channel_id=1, source_target_pairs={{0,1},{1,2},{2,3},{3,0},{4,5},{5,6},{6,7},{7,4},{8,9},{9,10},{10,1... | collective-permute-start | bytes 2359304 | tf_op jit(solution)/shard_map/ppermute | solution.py:117
  220.3 11.4 %collective-permute-start.1 = (bf16[512,768]{1,0:T(8,128)(2,1)S(1)}, bf16[512,768]{1,0:T(8,128)(2,1)S(1)}, u32[]{:S(2)}, u32[]{:S(2)}) collective-permute-start(bf16[512,768]{1,0:T(8,128)(2,1)S(1)} %collective-permute-done), channel_id=1, source_target_pairs={{0,1},{1,2},{2,3},{3,0},{4,5},{5,6},{6,7},{7,4},{8,9},{9,10},{10,1... | collective-permute-start | bytes 2359304 | tf_op jit(solution)/shard_map/ppermute | solution.py:117
  231.7 11.4 %collective-permute-start.2 = (bf16[512,768]{1,0:T(8,128)(2,1)S(1)}, bf16[512,768]{1,0:T(8,128)(2,1)S(1)}, u32[]{:S(2)}, u32[]{:S(2)}) collective-permute-start(bf16[512,768]{1,0:T(8,128)(2,1)S(1)} %collective-permute-done.1), channel_id=1, source_target_pairs={{0,1},{1,2},{2,3},{3,0},{4,5},{5,6},{6,7},{7,4},{8,9},{9,10},{10,1... | collective-permute-start | bytes 2359304 | tf_op jit(solution)/shard_map/ppermute | solution.py:117
  248.1 18.5 %copy-start.1 = (bf16[512,512]{0,1:T(8,128)(2,1)S(1)}, bf16[512,512]{0,1:T(8,128)(2,1)}, u32[]{:S(2)}) copy-start(bf16[512,512]{0,1:T(8,128)(2,1)} %add_convert_fusion.1) | copy-start | bytes 1572868
  248.1 18.5 %copy-start.16 = (f32[512]{0:T(512)S(1)}, f32[512]{0:T(512)}, u32[]{:S(2)}) copy-start(f32[512]{0:T(512)} %param.35) | copy-start | bytes 6148
Sparse Core Ops, SparseCore 0:
  8.9 25.2 all-gather.5
  35.8 78.6 all-gather.9
  116.0 22.1 all-gather.7
  139.6 63.4 all-gather.11
  204.5 62.0 all-gather.13
